TPU v7x, 32 devices: a whole 2x2x4 slice. The times are simulated.
32 devices in a mesh: fs: 8 (over z, x), tp: 4 (over y, core).
Axes of the slice: x: 2, y: 2, z: 4, core: 2. Of those that a mesh axis runs over, the one named last changes fastest.
Arguments:
- tokens: bfloat16 [8192, 2048], P(('fs', 'tp')), may hold values from -130 to 130
- pool_weight: bfloat16 [4, 512, 512], P(None, 'fs'), may hold values from -0.25 to 0.25
- pool_scale: float32 [2048], replicated, may hold values from 0.5 to 1.5
- gain_mix: float32 [2048], replicated, may hold values from 0.1 to 1.9
- gain_mlp: float32 [2048], replicated, may hold values from 0.1 to 1.9
- w_up: bfloat16 [8192, 2048], P('tp', 'fs'), may hold values from -0.125 to 0.125
- w_down: bfloat16 [8192, 2048], P('tp', 'fs'), may hold values from -0.0625 to 0.0625
- gain_out: float32 [2048], P('tp'), may hold values from 0.1 to 1.9
Outputs:
- result: bfloat16 [8192, 2048], P('fs', 'tp')
All inputs are finite; a program needn't handle non-finite values.
Results may differ from a plain program's by a relative error of at most 0.013.
Values may be sent and summed in bfloat16 or wider, within the bound.
A program may use at most 64 MiB of HBM per device.

v0:
```python
import jax
import jax.numpy as jnp
from jax import lax
from jax.sharding import PartitionSpec as P

D = 2048
SEQ_LEN = 1024


EPS = 1e-06
WINDOWS = (2, 4, 8, 16)


def extended_2(x, sides, width):
    for axis, dim in sides:
        peers, length = (lax.axis_size(axis), x.shape[dim])
        up = [(i, (i + 1) % peers) for i in range(peers - 1)]
        down = [(j, i) for i, j in up]
        last = lax.slice_in_dim(x, length - width, length, axis=dim)
        first = lax.slice_in_dim(x, 0, width, axis=dim)
        before = lax.ppermute(last, axis, up)
        after = lax.ppermute(first, axis, down)
        x = jnp.concatenate([before, x, after], axis=dim)
    return x


def rms_scale(values, gain):
    return values * lax.rsqrt(jnp.mean(values * values, axis=-1, keepdims=True) + EPS) * gain


def local(tokens, pool_weight, pool_scale, gain_mix, gain_mlp, w_up, w_down, gain_out):
    rows = tokens.shape[0]
    width = tokens.shape[1]
    group = width // 4
    offset = lax.axis_index("tp") * rows
    inputs = tokens.astype(jnp.float32)
    normed = rms_scale(inputs, gain_mix).astype(jnp.bfloat16)
    extended = extended_2(normed, (("tp", 0),), 8).astype(jnp.float32)
    line = jnp.arange(rows + 16, dtype=jnp.int32)
    lower_open = offset % SEQ_LEN != 0
    upper_open = (offset + rows) % SEQ_LEN != 0
    keep = jnp.where(line < 8, lower_open, jnp.where(line >= rows + 8, upper_open, True))
    level = extended * keep.astype(jnp.float32)[:, None]
    position = (offset + jnp.arange(rows, dtype=jnp.int32)) % SEQ_LEN
    normed_f32 = normed.astype(jnp.float32)
    full_pool = lax.all_gather(pool_weight, "fs", axis=1, tiled=True)
    pieces = []
    for index, reach in enumerate(WINDOWS):
        half = reach // 2
        level = level[:-half] + level[half:]
        start = 8 - half
        window = level[start : start + rows, :group]
        lower = jnp.maximum(position - half, 0)
        upper = jnp.minimum(position + half, SEQ_LEN)
        counts = (upper - lower).astype(jnp.float32)[:, None]
        own = normed_f32[:, index * group : (index + 1) * group]
        pooled = (window / counts - own).astype(jnp.bfloat16)
        pieces.append(jnp.dot(pooled, full_pool[index], preferred_element_type=jnp.float32))
        level = level[:, group:]
    mixed = jnp.concatenate(pieces, axis=1) * pool_scale
    first_sum = (inputs + mixed).astype(jnp.bfloat16)
    inner = rms_scale(first_sum.astype(jnp.float32), gain_mlp).astype(jnp.bfloat16)
    all_inner = lax.all_gather(inner, "tp", axis=0, tiled=True)
    contract = (((1,), (1,)), ((), ()))
    pre = lax.dot_general(
        all_inner,
        lax.all_gather(w_up, "fs", axis=1, tiled=True),
        contract,
        preferred_element_type=jnp.float32,
    )
    hidden = jnp.square(jax.nn.relu(pre)).astype(jnp.bfloat16)
    partial_terms = jnp.dot(
        hidden, lax.all_gather(w_down, "fs", axis=1, tiled=True), preferred_element_type=jnp.float32
    )
    channel_out = lax.psum_scatter(
        partial_terms.astype(jnp.bfloat16), "tp", scatter_dimension=1, tiled=True
    ).astype(jnp.float32)
    first_columns = lax.all_to_all(first_sum, "tp", split_axis=1, concat_axis=0, tiled=True)
    second_sum = first_columns.astype(jnp.float32) + channel_out
    squares = lax.psum(jnp.sum(second_sum * second_sum, axis=1), "tp")
    scaled = second_sum * lax.rsqrt(squares / D + EPS)[:, None] * gain_out
    return scaled.astype(jnp.bfloat16)


def solution(mesh):
    return jax.shard_map(
        local,
        mesh=mesh,
        in_specs=(
            P(("fs", "tp"), None),
            P(None, "fs", None),
            P(),
            P(),
            P(),
            P("tp", "fs"),
            P("tp", "fs"),
            P("tp"),
        ),
        out_specs=P("fs", "tp"),
        check_vma=False,
    )
```

profile of v0, /device:TPU:0, one launch (start us, length us, event | category | flops | bytes accessed | tf_op | source)
XLA Modules:
  0.0 437.5 jit_solution(9384960922146906074)
XLA Ops:
  6.5 0.7 all-gather.5.cloned.1.call-update
  7.3 1.5 fusion.3
  8.8 2.9 fusion.30
  11.7 2.4 collective-permute-start
  14.1 1.3 collective-permute-start.1
  15.5 3.8 collective-permute-done.1
  19.3 0.2 convert_multiply_fusion.4
  19.5 0.3 slice_add_fusion
  19.8 0.2 slice_add_fusion.1
  20.1 1.2 copy-done.1
  21.4 1.1 fusion.32
  22.6 38.8 %all-gather.5.cloned.1.call-done = bf16[4,512,512]{2,1,0:T(8,128)(2,1)} async-done(((bf16[4,64,512]{2,1,0:T(8,128)(2,1)}), bf16[4,512,512]{2,1,0:T(8,128)(2,1)}) %all-gather.5.cloned.1.call-update) | async-done | bytes 2097168 | tf_op jit(solution)/shard_map/all_gather | solution.py:46
  61.3 1.7 fusion.14
  63.1 0.2 copy-done.3
  63.2 1.7 fusion.12
  65.0 0.4 fusion.10
  65.4 0.6 copy-done.4
  66.2 0.4 fusion.7
  66.7 0.5 fusion
  67.2 0.2 copy-done.7
  67.4 1.3 fusion.2
  68.7 0.7 all-gather.9.cloned.1.call-update
  69.5 0.5 all-gather.11.cloned.1.call-update
  70.0 31.8 %all-gather.7.cloned.1.call-done = bf16[1024,2048]{1,0:T(8,128)(2,1)} async-done(((bf16[256,2048]{1,0:T(8,128)(2,1)}), bf16[1024,2048]{1,0:T(8,128)(2,1)}) %all-gather.7.cloned.1.call-update) | async-done | bytes 4194320 | tf_op jit(solution)/shard_map/all_gather | solution.py:63
  101.8 127.0 %all-gather.9.cloned.1.call-done = bf16[2048,2048]{1,0:T(8,128)(2,1)} async-done(((bf16[2048,256]{1,0:T(8,128)(2,1)}), bf16[2048,2048]{1,0:T(8,128)(2,1)}) %all-gather.9.cloned.1.call-update) | async-done | bytes 8388624 | tf_op jit(solution)/shard_map/all_gather | solution.py:67
  228.8 125.0 %all-gather.11.cloned.1.call-done = bf16[2048,2048]{1,0:T(8,128)(2,1)} async-done(((bf16[2048,256]{1,0:T(8,128)(2,1)}), bf16[2048,2048]{1,0:T(8,128)(2,1)}) %all-gather.11.cloned.1.call-update) | async-done | bytes 8388624 | tf_op jit(solution)/shard_map/all_gather | solution.py:73
  353.9 25.5 %convolution_convert_fusion = bf16[1024,2048]{1,0:T(8,128)(2,1)} fusion(bf16[2048,2048]{1,0:T(8,128)(2,1)} %all-gather.11.cloned.1.call-done, bf16[1024,2048]{1,0:T(8,128)(2,1)} %all-gather.7.cloned.1.call-done, bf16[2048,2048]{1,0:T(8,128)(2,1)} %all-gather.9.cloned.1.call-done), kind=kOutput, calls=%fused_computation.1 | convolution fusion | flops 17188257792 | bytes 25165824 | tf_op jit(solution)/shard_map/dot_general | solution.py:72
  379.5 17.0 %all_to_all.13 = bf16[256,4,512]{2,0,1:T(8,128)(2,1)S(1)} all-to-all(bf16[256,4,512]{2,0,1:T(8,128)(2,1)S(1)} %bitcast.28), channel_id=1, replica_groups=mesh['fs'=8,'tp'=4] {'tp'}, dimensions={1} | all-to-all | bytes 2097152 | tf_op jit(solution)/shard_map/all_to_all | solution.py:78
  396.5 25.6 %reduce-scatter.2.cloned.1.call-done = bf16[1024,512]{1,0:T(8,128)(2,1)} async-done(((bf16[1024,2048]{1,0:T(8,128)(2,1)}), bf16[1024,512]{1,0:T(8,128)(2,1)}) %reduce-scatter.2.cloned.1.call-update) | async-done | bytes 1048592 | tf_op jit(solution)/shard_map/reduce_scatter | solution.py:75
  422.1 1.7 multiply_reduce_fusion
  423.8 5.8 %psum.7 = f32[1024]{0:T(1024)S(1)} all-reduce(f32[1024]{0:T(1024)S(1)} %multiply_reduce_fusion), channel_id=1, replica_groups=mesh['fs'=8,'tp'=4] {'tp'}, use_global_device_ids=true, to_apply=%region_4.5 | all-reduce | flops 1024 | bytes 8192 | tf_op jit(solution)/shard_map/psum | solution.py:80
  429.6 1.4 multiply_convert_fusion.1
  (33 shorter events, 0.9 us)
Async XLA Ops:
  6.5 54.8 %all-gather.5.cloned.1.call-start = ((), (), s32[]{:S(2)}) async-start(), calls=%async_computation.2 | async-start | bytes 2359296 | tf_op jit(solution)/shard_map/all_gather | solution.py:46
  7.3 94.6 %all-gather.7.cloned.1.call-start = ((), (), s32[]{:S(2)}) async-start(), calls=%async_computation.3 | async-start | bytes 5242880 | tf_op jit(solution)/shard_map/all_gather | solution.py:63
  11.7 3.8 collective-permute-start
  14.1 5.2 %collective-permute-start.1 = (bf16[8,2048]{1,0:T(8,128)(2,1)S(1)}, bf16[8,2048]{1,0:T(8,128)(2,1)S(1)}, u32[]{:S(2)}, u32[]{:S(2)}) collective-permute-start(bf16[8,2048]{1,0:T(8,128)(2,1)S(1)} %get-tuple-element.12), channel_id=1, source_target_pairs={{1,0},{2,1},{3,2},{5,4},{6,5},{7,6},{9,8},{10,9},{11,10},{13,12},{... | collective-permute-start | bytes 98312 | tf_op jit(solution)/shard_map/ppermute | solution.py:22
  20.1 1.2 copy-start.1
  61.3 1.9 copy-start.3
  63.0 2.0 copy-start.9
  64.9 1.1 copy-start.4
  64.9 1.2 copy-start.5
  65.4 1.3 copy-start
  65.4 1.3 copy-start.6
  66.7 0.7 copy-start.7
  68.7 160.2 %all-gather.9.cloned.1.call-start = ((), (), s32[]{:S(2)}) async-start(), calls=%async_computation.4 | async-start | bytes 9437184 | tf_op jit(solution)/shard_map/all_gather | solution.py:67
  69.4 284.5 %all-gather.11.cloned.1.call-start = ((), (), s32[]{:S(2)}) async-start(), calls=%async_computation.5 | async-start | bytes 9437184 | tf_op jit(solution)/shard_map/all_gather | solution.py:73
  70.0 352.1 %reduce-scatter.2.cloned.1.call-start = ((), (), s32[]{:S(2)}) async-start(), calls=%async_computation.6 | async-start | bytes 5242880 | tf_op jit(solution)/shard_map/reduce_scatter | solution.py:75
  379.5 50.1 %copy-start.8 = (f32[512]{0:T(512)S(1)}, f32[512]{0:T(512)}, u32[]{:S(2)}) copy-start(f32[512]{0:T(512)} %param.15) | copy-start | bytes 6148
  422.1 7.5 %copy-start.2 = (bf16[1024,512]{1,0:T(8,128)(2,1)S(1)}, bf16[1024,512]{1,0:T(8,128)(2,1)}, u32[]{:S(2)}) copy-start(bf16[1024,512]{1,0:T(8,128)(2,1)} %reduce-scatter.2.cloned.1.call-done) | copy-start | bytes 3145732
Sparse Core Ops, SparseCore 0:
  9.5 51.7 all-gather.4
  68.8 32.9 all-gather.6
  103.9 124.9 all-gather.8
  230.7 123.1 all-gather.10
  379.5 42.5 reduce-scatter.1
where the time goes:
time: 438 us
  waiting for transfers between devices  354 us (81%)
  matrix products  29.5 us (7%)
  blocking collectives  22.8 us (5%)
  between operations  13.3 us (3%)
  other arithmetic  10.2 us (2%)
    all_gather x1, waiting for transfers between devices, local(): lax.all_gather(w_up, 'fs', axis=1, tiled=True)  127 us
    all_gather x1, waiting for transfers between devices, local(): lax.all_gather(w_down, 'fs', axis=1, tiled=True)  125 us
    all_gather x1, waiting for transfers between devices, local(): full_pool = lax.all_gather(pool_weight, 'fs', axis=1, tiled=True)  38.8 us
    all_gather x1, waiting for transfers between devices, local(): all_inner = lax.all_gather(inner, 'tp', axis=0, tiled=True)  31.8 us
    reduce_scatter x1, waiting for transfers between devices, local(): lax.psum_scatter(partial_terms.astype(jnp.bfloat16), 'tp', scatter_dimens...  25.6 us
    dot_general x1, matrix products, local(): jnp.dot(hidden, lax.all_gather(w_down, 'fs', axis=1, tiled=True), preferr...  25.5 us
    all_to_all x1, blocking collectives, local(): lax.all_to_all(first_sum, 'tp', split_axis=1, concat_axis=0, tiled=True)  17 us
  transfers between devices with their start and end apart: 7, of which 6 were waited for; matrix products, arithmetic and copies ran while one was open for 1% of the time, Pallas kernels for 0%

commit v1 on v0

v1 whole, which is shorter than its diff:
```python
import functools

import jax
import jax.numpy as jnp
from jax import lax
from jax.experimental import pallas as pl
from jax.experimental.pallas import tpu as pltpu
from jax.sharding import PartitionSpec as P

SEQ_LEN = 1024
EPS = 1e-06
WINDOWS = (2, 4, 8, 16)
HALO = 16
MESH = pl.DeviceIdType.MESH
POOL, UP, DOWN = 0, 1, 2


def ring_order(n, nx):
    nz = n // nx
    if nx < 2 or nz < 2 or nz % 2:
        return list(range(n))
    order = []
    for z in range(nz):
        xs = list(range(1, nx))
        order += [z * nx + x for x in (xs if z % 2 == 0 else xs[::-1])]
    return order + [z * nx for z in range(nz - 1, -1, -1)]


def lookup(table, index):
    value = jnp.int32(table[0])
    for i in range(1, len(table)):
        value = jnp.where(index == i, jnp.int32(table[i]), value)
    return value


def kernel(
    n, tp, order, tok_ref, pool_ref, up_ref, down_ref, scale_ref, gmix_ref, gmlp_ref, out_ref,
    pool_full, up_full, down_full, ext, first, inner_all, hidden, fcols, blocks, parts,
    before, after, edge,
    ring_send, ring_recv, in_send, in_recv, fc_send, fc_recv, halo_send, halo_recv, rs_send, rs_recv,
):
    rows, width = tok_ref.shape
    group = width // 4
    hid, cols = up_ref.shape
    depth = pool_ref.shape[1]
    own_cols = width // tp
    per = n // tp
    seq = rows * tp
    me_fs, me = lax.axis_index("fs"), lax.axis_index("tp")
    place_of = [order.index(i) for i in range(n)]
    place = lookup(place_of, me_fs)

    def at(offset):
        return lookup(order, lax.rem(place + offset + 2 * n, n))

    owners = {0: me_fs}
    for d in range(1, n // 2 + 1):
        owners[d] = at(d)
        owners[-d] = at(-d)
    right, left = owners[1], owners[-1]

    barrier = pltpu.get_barrier_semaphore()
    for peer in (right, left):
        pl.semaphore_signal(barrier, inc=1, device_id={"fs": peer, "tp": me}, device_id_type=MESH)
    for d in range(1, tp):
        pl.semaphore_signal(
            barrier, inc=1, device_id={"fs": me_fs, "tp": lax.rem(me + d, tp)}, device_id_type=MESH
        )
    pl.semaphore_wait(barrier, 2 + tp - 1)

    hops = n // 2

    def view(stream, full, owner, piece):
        if stream == POOL:
            ref = pool_full if full else pool_ref
            half = ref.shape[0] // 2
            r = pl.ds(pl.multiple_of(owner * depth, depth), depth) if full else slice(None)
            return ref.at[pl.ds(piece * half, half), r, :]
        ref = (up_full if full else up_ref) if stream == UP else (down_full if full else down_ref)
        half = hid // 2
        c = pl.ds(pl.multiple_of(owner * cols, cols), cols) if full else slice(None)
        return ref.at[pl.ds(piece * half, half), c]

    def count(side, piece):
        return hops if piece == side else hops - 1

    def ring(stream, side, piece, hop):
        owner = owners[-hop] if side == 0 else owners[hop]
        return pltpu.make_async_remote_copy(
            src_ref=view(stream, hop > 0, owner, piece),
            dst_ref=view(stream, True, owner, piece),
            send_sem=ring_send.at[((stream * 2 + side) * 2 + piece) * hops + hop],
            recv_sem=ring_recv.at[((stream * 2 + side) * 2 + piece) * hops + hop],
            device_id={"fs": right if side == 0 else left, "tp": me},
            device_id_type=MESH,
        )

    started = []

    def arrived(stream, side, piece, hop):
        owner = owners[-hop - 1] if side == 0 else owners[hop + 1]
        pltpu.make_async_remote_copy(
            src_ref=view(stream, True, owner, piece),
            dst_ref=view(stream, True, owner, piece),
            send_sem=ring_send.at[((stream * 2 + side) * 2 + piece) * hops + hop],
            recv_sem=ring_recv.at[((stream * 2 + side) * 2 + piece) * hops + hop],
            device_id={"fs": right if side == 0 else left, "tp": me},
            device_id_type=MESH,
        ).wait_recv()

    def start(stream, hop, which=(0, 1)):
        for w in which:
            for side in (0, 1):
                piece = side if w == 0 else 1 - side
                if hop < count(side, piece):
                    if hop > 0:
                        arrived(stream, side, piece, hop - 1)
                    copy = ring(stream, side, piece, hop)
                    copy.start()
                    started.append(copy)

    def finish(stream):
        for side in (0, 1):
            piece = side
            arrived(stream, side, piece, hops - 1)

    def settle(stream, hop):
        if hop == hops - 2:
            for side in (0, 1):
                arrived(stream, side, 1 - side, hop)

    start(POOL, 0)
    start(UP, 0, (0,))

    step = 32 if rows % 32 == 0 else rows

    @pl.loop(0, rows // step)
    def _(i):
        r = pl.ds(pl.multiple_of(i * step, step), step)
        x = tok_ref[r, :].astype(jnp.float32)
        y = x * lax.rsqrt(jnp.mean(x * x, axis=-1, keepdims=True) + EPS) * gmix_ref[...]
        y = y.astype(jnp.bfloat16)
        ext[pl.ds(pl.multiple_of(HALO + i * step, HALO), step), :] = y.astype(jnp.float32)

    edge[0] = ext[rows : rows + HALO, :].astype(jnp.bfloat16)
    edge[1] = ext[HALO : 2 * HALO, :].astype(jnp.bfloat16)
    halos = []
    for side, (buffer, d) in enumerate(((before, 1), (after, tp - 1))):
        copy = pltpu.make_async_remote_copy(
            src_ref=edge.at[side],
            dst_ref=buffer,
            send_sem=halo_send.at[side],
            recv_sem=halo_recv.at[side],
            device_id={"fs": me_fs, "tp": lax.rem(me + d, tp)},
            device_id_type=MESH,
        )
        copy.start()
        halos.append(copy)

    start(POOL, 1)
    start(UP, 0, (1,))
    for hop in range(2, hops):
        start(POOL, hop)
    pool_full[:, pl.ds(pl.multiple_of(me_fs * depth, depth), depth), :] = pool_ref[...]
    mine = pl.ds(pl.multiple_of(me_fs * cols, cols), cols)
    up_full[:, mine] = up_ref[...]
    down_full[:, mine] = down_ref[...]
    for copy in halos:
        copy.wait()
    offset = me * rows
    lower_open = (lax.rem(offset, SEQ_LEN) != 0).astype(jnp.float32)
    upper_open = (lax.rem(offset + rows, SEQ_LEN) != 0).astype(jnp.float32)
    ext[0:HALO, :] = before[...].astype(jnp.float32) * lower_open
    ext[rows + HALO : rows + 2 * HALO, :] = after[...].astype(jnp.float32) * upper_open
    start(UP, 1)
    settle(POOL, hops - 2)
    finish(POOL)

    position = lax.rem(offset + lax.broadcasted_iota(jnp.int32, (rows, 1), 0), SEQ_LEN)
    for index, reach in enumerate(WINDOWS):
        half = reach // 2
        c = slice(index * group, (index + 1) * group)
        level = ext[:, c]
        own = level[HALO : HALO + rows]
        shift = 1
        while shift < reach:
            level = level + pltpu.roll(level, shift, 0)
            shift *= 2
        if half > 1:
            level = pltpu.roll(level, rows + 2 * HALO - (half - 1), 0)
        window = level[HALO : HALO + rows]
        counts = (jnp.minimum(position + half, SEQ_LEN) - jnp.maximum(position - half, 0)).astype(jnp.float32)
        pooled = (window / counts - own).astype(jnp.bfloat16)
        mixed = jnp.dot(pooled, pool_full[index], preferred_element_type=jnp.float32)
        first[:, c] = (tok_ref[:, c].astype(jnp.float32) + mixed * scale_ref[:, c]).astype(jnp.bfloat16)
    for hop in range(2, 3):
        if hop < hops:
            start(UP, hop)

    @pl.loop(0, rows // step)
    def _(i):
        r = pl.ds(pl.multiple_of(i * step, step), step)
        x = first[r, :].astype(jnp.float32)
        y = x * lax.rsqrt(jnp.mean(x * x, axis=-1, keepdims=True) + EPS) * gmlp_ref[...]
        inner_all[pl.ds(pl.multiple_of(me * rows + i * step, step), step), :] = y.astype(jnp.bfloat16)

    my_rows = pl.ds(pl.multiple_of(me * rows, rows), rows)
    inners, firsts = [], []
    for d in range(1, tp):
        peer = lax.rem(me + d, tp)
        copy = pltpu.make_async_remote_copy(
            src_ref=inner_all.at[my_rows, :],
            dst_ref=inner_all.at[my_rows, :],
            send_sem=in_send.at[d],
            recv_sem=in_recv.at[d],
            device_id={"fs": me_fs, "tp": peer},
            device_id_type=MESH,
        )
        copy.start()
        inners.append(copy)
    for d in range(1, tp):
        peer = lax.rem(me + d, tp)
        copy = pltpu.make_async_remote_copy(
            src_ref=first.at[:, pl.ds(pl.multiple_of(peer * own_cols, own_cols), own_cols)],
            dst_ref=fcols.at[my_rows, :],
            send_sem=fc_send.at[d],
            recv_sem=fc_recv.at[d],
            device_id={"fs": me_fs, "tp": peer},
            device_id_type=MESH,
        )
        copy.start()
        firsts.append(copy)
    fcols[my_rows, :] = first[:, pl.ds(pl.multiple_of(me * own_cols, own_cols), own_cols)]

    for hop in range(3, hops):
        start(UP, hop)
    settle(UP, hops - 2)
    start(DOWN, 0)
    finish(UP)
    for d in range(1, tp):
        source = pl.ds(pl.multiple_of(lax.rem(me + tp - d, tp) * rows, rows), rows)
        pltpu.make_async_remote_copy(
            src_ref=inner_all.at[source, :],
            dst_ref=inner_all.at[source, :],
            send_sem=in_send.at[d],
            recv_sem=in_recv.at[d],
            device_id={"fs": me_fs, "tp": lax.rem(me + d, tp)},
            device_id_type=MESH,
        ).wait_recv()

    tile = min(256, hid)

    @pl.loop(0, hid // tile)
    def _(j):
        h = pl.ds(pl.multiple_of(j * tile, tile), tile)
        pre = lax.dot_general(
            inner_all[...], up_full[h, :], (((1,), (1,)), ((), ())), preferred_element_type=jnp.float32
        )
        hidden[:, h] = jnp.square(jnp.maximum(pre, 0.0)).astype(jnp.bfloat16)

    sums = []

    def block(k, owner):
        c = pl.ds(pl.multiple_of(owner * cols, cols), cols)
        part = min(512, seq)

        @pl.loop(0, seq // part)
        def _(i):
            r = pl.ds(pl.multiple_of(i * part, part), part)
            blocks[k, r, :] = jnp.dot(
                hidden[r, :], down_full[:, c], preferred_element_type=jnp.float32
            ).astype(jnp.bfloat16)

        dest = owner // per
        d = lax.rem(dest - me + tp, tp)
        local = lax.rem(owner, per)
        lc = pl.ds(pl.multiple_of(local * cols, cols), cols)

        @pl.when(d == 0)
        def _():
            parts[0, :, lc] = blocks[k]

        copy = pltpu.make_async_remote_copy(
            src_ref=blocks.at[k],
            dst_ref=parts.at[d, :, lc],
            send_sem=rs_send.at[k],
            recv_sem=rs_recv.at[d * per + local],
            device_id={"fs": me_fs, "tp": dest},
            device_id_type=MESH,
        )

        @pl.when(d != 0)
        def _():
            copy.start()

        sums.append((d, copy))

    block(0, owners[0])
    k = 1
    for hop in range(1, hops):
        start(DOWN, hop)
        settle(DOWN, hop - 1)
        if hop == hops - 1:
            for side in (0, 1):
                pass
        for owner in (owners[-hop], owners[hop]):
            block(k, owner)
            k += 1
    finish(DOWN)
    block(k, owners[hops])

    for copy in started:
        copy.wait_send()
    for copy in inners:
        copy.wait_send()
    for copy in firsts:
        copy.wait()
    for d, copy in sums:
        @pl.when(d != 0)
        def _(copy=copy):
            copy.wait_send()
    for d in range(1, tp):
        for local in range(per):
            lc = pl.ds(local * cols, cols)
            pltpu.make_async_remote_copy(
                src_ref=blocks.at[0],
                dst_ref=parts.at[d, :, lc],
                send_sem=rs_send.at[0],
                recv_sem=rs_recv.at[d * per + local],
                device_id={"fs": me_fs, "tp": lax.rem(me + d, tp)},
                device_id_type=MESH,
            ).wait_recv()

    @pl.loop(0, seq // 64)
    def _(i):
        r = pl.ds(pl.multiple_of(i * 64, 64), 64)
        total = parts[0, r, :].astype(jnp.float32)
        for d in range(1, tp):
            total = total + parts[d, r, :].astype(jnp.float32)
        out_ref[r, :] = fcols[r, :].astype(jnp.float32) + total


def local(order, tokens, pool_weight, pool_scale, gain_mix, gain_mlp, w_up, w_down, gain_out):
    n, tp = lax.axis_size("fs"), lax.axis_size("tp")
    rows, width = tokens.shape
    hid, cols = w_up.shape
    seq, own = rows * tp, width // tp
    bf, f32 = jnp.bfloat16, jnp.float32
    vmem = pl.BlockSpec(memory_space=pltpu.VMEM)
    dma = pltpu.SemaphoreType.DMA
    second_sum = pl.pallas_call(
        functools.partial(kernel, n, tp, order),
        out_shape=jax.ShapeDtypeStruct((seq, own), f32),
        in_specs=[vmem] * 7,
        out_specs=vmem,
        scratch_shapes=[
            pltpu.VMEM((pool_weight.shape[0], pool_weight.shape[1] * n, pool_weight.shape[2]), bf),
            pltpu.VMEM((hid, width), bf),
            pltpu.VMEM((hid, width), bf),
            pltpu.VMEM((rows + 2 * HALO, width), f32),
            pltpu.VMEM((rows, width), bf),
            pltpu.VMEM((seq, width), bf),
            pltpu.VMEM((seq, hid), bf),
            pltpu.VMEM((seq, own), bf),
            pltpu.VMEM((n, seq, cols), bf),
            pltpu.VMEM((tp, seq, own), bf),
            pltpu.VMEM((HALO, width), bf),
            pltpu.VMEM((HALO, width), bf),
            pltpu.VMEM((2, HALO, width), bf),
            dma((12 * (n // 2),)),
            dma((12 * (n // 2),)),
            dma((tp,)),
            dma((tp,)),
            dma((tp,)),
            dma((tp,)),
            dma((2,)),
            dma((2,)),
            dma((n,)),
            dma((n,)),
        ],
        compiler_params=pltpu.CompilerParams(
            collective_id=0, has_side_effects=True, vmem_limit_bytes=63 * 1024 * 1024
        ),
    )(
        tokens, pool_weight, w_up, w_down,
        pool_scale.reshape(1, -1), gain_mix.reshape(1, -1), gain_mlp.reshape(1, -1),
    )
    squares = lax.psum(jnp.sum(second_sum * second_sum, axis=1), "tp")
    scaled = second_sum * lax.rsqrt(squares / width + EPS)[:, None] * gain_out
    return scaled.astype(jnp.bfloat16)


def grid_width(mesh):
    n = mesh.shape["fs"]
    try:
        line = mesh.devices.reshape(n, -1)[:, 0]
        nx = len({d.coords[0] for d in line})
        if n % nx == 0:
            return nx
    except AttributeError:
        pass
    return 2 if n % 2 == 0 else 1


def solution(mesh):
    order = ring_order(mesh.shape["fs"], grid_width(mesh))
    return jax.shard_map(
        functools.partial(local, order),
        mesh=mesh,
        in_specs=(
            P(("fs", "tp"), None),
            P(None, "fs", None),
            P(),
            P(),
            P(),
            P("tp", "fs"),
            P("tp", "fs"),
            P("tp"),
        ),
        out_specs=P("fs", "tp"),
        check_vma=False,
    )
```

time: 438 us -> 216 us (0.49)
  waiting for transfers between devices: 354 us -> 0 us
  Pallas kernels: 0 us -> 192 us
  matrix products: 29.5 us -> 0 us
  between operations: 13.3 us -> 0.03 us
  other arithmetic: 10.2 us -> 3.18 us
    all_gather x4 -> x0, waiting for transfers between devices: 323 us -> none  [the longest x1 127 us: local(): lax.all_gather(w_up, 'fs', axis=1, tiled=True)]
    pallas_call x0 -> x1, Pallas kernels: none -> 192 us  [local(): pl.pallas_call(functools.partial(kernel, n, tp, order), out_shape=jax.Sha...]
    dot_general x5 -> x0, matrix products: 29.5 us -> none  [the longest x1 25.5 us: local(): jnp.dot(hidden, lax.all_gather(w_down, 'fs', axis=1, tiled=True), preferr...]
    reduce_scatter x1 -> x0, waiting for transfers between devices: 25.6 us -> none  [local(): lax.psum_scatter(partial_terms.astype(jnp.bfloat16), 'tp', scatter_dimens...]
    all_to_all x1 -> x0, blocking collectives: 17 us -> none  [local(): lax.all_to_all(first_sum, 'tp', split_axis=1, concat_axis=0, tiled=True)]
    psum x1, blocking collectives: 5.77 us -> 20.4 us  [local(): squares = lax.psum(jnp.sum(second_sum * second_sum, axis=1), 'tp')]
  transfers between devices with their start and end apart: 7 -> 0, of which waited for: 6 -> 0; matrix products, arithmetic and copies ran while one was open for 1% -> 0% of each run, Pallas kernels for 0% -> 0%
where the time goes in v1:
time: 216 us; the launch traced here: 215 us
  Pallas kernels  192 us (89%)
  blocking collectives  20.4 us (9%)
  other arithmetic  3.18 us (1%)
    pallas_call x1, Pallas kernels, local(): pl.pallas_call(functools.partial(kernel, n, tp, order), out_shape=jax.Sha...  192 us
    psum x1, blocking collectives, local(): squares = lax.psum(jnp.sum(second_sum * second_sum, axis=1), 'tp')  20.4 us

profile of v1, /device:TPU:0, one launch (start us, length us, event | category | flops | bytes accessed | tf_op | source)
XLA Modules:
  0.0 215.4 jit_solution(14903247401326230336)
XLA Ops:
  0.0 191.7 %shard_map.82 = f32[1024,512]{1,0:T(8,128)} custom-call(bf16[256,2048]{1,0:T(8,128)(2,1)} %tok_ref.1, bf16[4,64,512]{2,1,0:T(8,128)(2,1)} %pool_ref.1, bf16[2048,256]{1,0:T(8,128)(2,1)} %up_ref.1, bf16[2048,256]{1,0:T(8,128)(2,1)} %down_ref.1, f32[1,2048]{1,0:T(1,128)} %bitcast.3, f32[1,2048]{1,0:T(1,128)} %bitcast.4, f32[1,2048]{1,0:T(1,128)} %bitcast.5), custom_call_target="tpu_custom_call" | custom-call | tf_op jit(solution)/shard_map/pallas_call | solution.py:351
  191.7 0.0 copy-start
  191.7 0.0 copy-start.1
  191.8 2.0 multiply_reduce_fusion
  193.7 20.4 %psum.7 = f32[1024]{0:T(1024)S(1)} all-reduce(f32[1024]{0:T(1024)S(1)} %multiply_reduce_fusion), channel_id=1, replica_groups=mesh['fs'=8,'tp'=4] {'tp'}, use_global_device_ids=true, to_apply=%region_1.0 | all-reduce | flops 1024 | bytes 8192 | tf_op jit(solution)/shard_map/psum | solution.py:388
  214.2 0.0 copy-done
  214.2 0.0 copy-done.1
  214.2 1.2 multiply_convert_fusion
  (1 shorter events, 0.0 us)
Async XLA Ops:
  191.7 22.4 %copy-start = (f32[1024,512]{1,0:T(8,128)S(1)}, f32[1024,512]{1,0:T(8,128)}, u32[]{:S(2)}) copy-start(f32[1024,512]{1,0:T(8,128)} %shard_map.82) | copy-start | bytes 6291460
  191.7 22.4 %copy-start.1 = (f32[512]{0:T(512)S(1)}, f32[512]{0:T(512)}, u32[]{:S(2)}) copy-start(f32[512]{0:T(512)} %param.15) | copy-start | bytes 6148

commit v2 on v1

--- a/solution.py
+++ b/solution.py
@@ -34,10 +34,12 @@
 
 
 def kernel(
-    n, tp, order, tok_ref, pool_ref, up_ref, down_ref, scale_ref, gmix_ref, gmlp_ref, out_ref,
+    n, tp, order, tok_ref, pool_ref, up_ref, down_ref, scale_ref, gmix_ref, gmlp_ref,
+    gout_ref, out_ref,
     pool_full, up_full, down_full, ext, first, inner_all, hidden, fcols, blocks, parts,
-    before, after, edge,
+    before, after, edge, total, stat, stat_out, stat_in,
     ring_send, ring_recv, in_send, in_recv, fc_send, fc_recv, halo_send, halo_recv, rs_send, rs_recv,
+    pair_send, pair_recv, st_send, st_recv,
 ):
     rows, width = tok_ref.shape
     group = width // 4
@@ -69,41 +71,55 @@
     pl.semaphore_wait(barrier, 2 + tp - 1)
 
     hops = n // 2
-
-    def view(stream, full, owner, piece):
+    cores = 2 if tp % 2 == 0 else 1
+    core = lax.rem(me, cores)
+    lanes = 2 if cols % 256 == 0 else 1
+    fine = cols // lanes
+
+    def view(stream, full, owner, piece, sub=None):
         if stream == POOL:
             ref = pool_full if full else pool_ref
-            half = ref.shape[0] // 2
+            half = ref.shape[0] // (2 * cores)
             r = pl.ds(pl.multiple_of(owner * depth, depth), depth) if full else slice(None)
-            return ref.at[pl.ds(piece * half, half), r, :]
+            return ref.at[pl.ds((core * 2 + piece) * half, half), r, :]
         ref = (up_full if full else up_ref) if stream == UP else (down_full if full else down_ref)
         half = hid // 2
         c = pl.ds(pl.multiple_of(owner * cols, cols), cols) if full else slice(None)
+        if sub is not None:
+            c = pl.ds(pl.multiple_of(owner * cols + sub * fine, fine), fine)
         return ref.at[pl.ds(piece * half, half), c]
 
     def count(side, piece):
         return hops if piece == side else hops - 1
 
-    def ring(stream, side, piece, hop):
+    def slot(stream, side, piece, hop, sub):
+        if sub:
+            return 12 * hops + side * (lanes - 1) + sub - 1
+        return ((stream * 2 + side) * 2 + piece) * hops + hop
+
+    def subs(stream, hop):
+        return range(lanes) if stream == DOWN and hop == hops - 1 and hop > 0 else (None,)
+
+    def ring(stream, side, piece, hop, sub):
         owner = owners[-hop] if side == 0 else owners[hop]
         return pltpu.make_async_remote_copy(
-            src_ref=view(stream, hop > 0, owner, piece),
-            dst_ref=view(stream, True, owner, piece),
-            send_sem=ring_send.at[((stream * 2 + side) * 2 + piece) * hops + hop],
-            recv_sem=ring_recv.at[((stream * 2 + side) * 2 + piece) * hops + hop],
+            src_ref=view(stream, hop > 0, owner, piece, sub),
+            dst_ref=view(stream, True, owner, piece, sub),
+            send_sem=ring_send.at[slot(stream, side, piece, hop, sub)],
+            recv_sem=ring_recv.at[slot(stream, side, piece, hop, sub)],
             device_id={"fs": right if side == 0 else left, "tp": me},
             device_id_type=MESH,
         )
 
     started = []
 
-    def arrived(stream, side, piece, hop):
+    def arrived(stream, side, piece, hop, sub=None):
         owner = owners[-hop - 1] if side == 0 else owners[hop + 1]
         pltpu.make_async_remote_copy(
-            src_ref=view(stream, True, owner, piece),
-            dst_ref=view(stream, True, owner, piece),
-            send_sem=ring_send.at[((stream * 2 + side) * 2 + piece) * hops + hop],
-            recv_sem=ring_recv.at[((stream * 2 + side) * 2 + piece) * hops + hop],
+            src_ref=view(stream, True, owner, piece, sub),
+            dst_ref=view(stream, True, owner, piece, sub),
+            send_sem=ring_send.at[slot(stream, side, piece, hop, sub)],
+            recv_sem=ring_recv.at[slot(stream, side, piece, hop, sub)],
             device_id={"fs": right if side == 0 else left, "tp": me},
             device_id_type=MESH,
         ).wait_recv()
@@ -115,14 +131,14 @@
                 if hop < count(side, piece):
                     if hop > 0:
                         arrived(stream, side, piece, hop - 1)
-                    copy = ring(stream, side, piece, hop)
-                    copy.start()
-                    started.append(copy)
-
-    def finish(stream):
+                    for sub in subs(stream, hop):
+                        copy = ring(stream, side, piece, hop, sub)
+                        copy.start()
+                        started.append(copy)
+
+    def finish(stream, sub=None):
         for side in (0, 1):
-            piece = side
-            arrived(stream, side, piece, hops - 1)
+            arrived(stream, side, side, hops - 1, sub)
 
     def settle(stream, hop):
         if hop == hops - 2:
@@ -161,7 +177,8 @@
     start(UP, 0, (1,))
     for hop in range(2, hops):
         start(POOL, hop)
-    pool_full[:, pl.ds(pl.multiple_of(me_fs * depth, depth), depth), :] = pool_ref[...]
+    share = pl.ds(core * (pool_full.shape[0] // cores), pool_full.shape[0] // cores)
+    pool_full[share, pl.ds(pl.multiple_of(me_fs * depth, depth), depth), :] = pool_ref[share, :, :]
     mine = pl.ds(pl.multiple_of(me_fs * cols, cols), cols)
     up_full[:, mine] = up_ref[...]
     down_full[:, mine] = down_ref[...]
@@ -175,6 +192,25 @@
     start(UP, 1)
     settle(POOL, hops - 2)
     finish(POOL)
+    if cores > 1:
+        swap = pltpu.make_async_remote_copy(
+            src_ref=pool_full.at[share],
+            dst_ref=pool_full.at[share],
+            send_sem=pair_send,
+            recv_sem=pair_recv,
+            device_id={"fs": me_fs, "tp": me + 1 - 2 * core},
+            device_id_type=MESH,
+        )
+        swap.start()
+        other = pl.ds((1 - core) * (pool_full.shape[0] // cores), pool_full.shape[0] // cores)
+        pltpu.make_async_remote_copy(
+            src_ref=pool_full.at[other],
+            dst_ref=pool_full.at[other],
+            send_sem=pair_send,
+            recv_sem=pair_recv,
+            device_id={"fs": me_fs, "tp": me + 1 - 2 * core},
+            device_id_type=MESH,
+        ).wait_recv()
 
     position = lax.rem(offset + lax.broadcasted_iota(jnp.int32, (rows, 1), 0), SEQ_LEN)
     for index, reach in enumerate(WINDOWS):
@@ -259,35 +295,33 @@
         hidden[:, h] = jnp.square(jnp.maximum(pre, 0.0)).astype(jnp.bfloat16)
 
     sums = []
-
-    def block(k, owner):
-        c = pl.ds(pl.multiple_of(owner * cols, cols), cols)
-        part = min(512, seq)
+    part = min(512, seq)
+
+    def block(k, owner, sub):
+        c = pl.ds(pl.multiple_of(owner * cols + sub * fine, fine), fine)
 
         @pl.loop(0, seq // part)
         def _(i):
             r = pl.ds(pl.multiple_of(i * part, part), part)
-            blocks[k, r, :] = jnp.dot(
+            blocks[k, sub, r, :] = jnp.dot(
                 hidden[r, :], down_full[:, c], preferred_element_type=jnp.float32
             ).astype(jnp.bfloat16)
 
         dest = owner // per
         d = lax.rem(dest - me + tp, tp)
         local = lax.rem(owner, per)
-        lc = pl.ds(pl.multiple_of(local * cols, cols), cols)
+        copy = pltpu.make_async_remote_copy(
+            src_ref=blocks.at[k, sub],
+            dst_ref=parts.at[d, local, sub],
+            send_sem=rs_send.at[k * lanes + sub],
+            recv_sem=rs_recv.at[(d * per + local) * lanes + sub],
+            device_id={"fs": me_fs, "tp": dest},
+            device_id_type=MESH,
+        )
 
         @pl.when(d == 0)
         def _():
-            parts[0, :, lc] = blocks[k]
-
-        copy = pltpu.make_async_remote_copy(
-            src_ref=blocks.at[k],
-            dst_ref=parts.at[d, :, lc],
-            send_sem=rs_send.at[k],
-            recv_sem=rs_recv.at[d * per + local],
-            device_id={"fs": me_fs, "tp": dest},
-            device_id_type=MESH,
-        )
+            parts[0, local, sub] = blocks[k, sub]
 
         @pl.when(d != 0)
         def _():
@@ -295,49 +329,91 @@
 
         sums.append((d, copy))
 
-    block(0, owners[0])
+    def add_up(local, sub):
+        for d in range(1, tp):
+            pltpu.make_async_remote_copy(
+                src_ref=blocks.at[0, sub],
+                dst_ref=parts.at[d, local, sub],
+                send_sem=rs_send.at[0],
+                recv_sem=rs_recv.at[(d * per + local) * lanes + sub],
+                device_id={"fs": me_fs, "tp": lax.rem(me + d, tp)},
+                device_id_type=MESH,
+            ).wait_recv()
+        c = pl.ds(pl.multiple_of(local * cols + sub * fine, fine), fine)
+
+        @pl.loop(0, seq // 128)
+        def _(i):
+            r = pl.ds(pl.multiple_of(i * 128, 128), 128)
+            value = parts[0, local, sub, r, :].astype(jnp.float32)
+            for d in range(1, tp):
+                value = value + parts[d, local, sub, r, :].astype(jnp.float32)
+            value = value + fcols[r, c].astype(jnp.float32)
+            total[r, c] = value
+            square = value * value
+            lump = square[:, 0:128]
+            for j in range(1, fine // 128):
+                lump = lump + square[:, j * 128 : (j + 1) * 128]
+            stat[r, :] = stat[r, :] + lump
+
+    for sub in range(lanes):
+        block(0, owners[0], sub)
+    stat[...] = jnp.zeros_like(stat)
     k = 1
     for hop in range(1, hops):
         start(DOWN, hop)
         settle(DOWN, hop - 1)
-        if hop == hops - 1:
-            for side in (0, 1):
-                pass
         for owner in (owners[-hop], owners[hop]):
-            block(k, owner)
+            for sub in range(lanes):
+                block(k, owner, sub)
             k += 1
-    finish(DOWN)
-    block(k, owners[hops])
-
+    for copy in firsts:
+        copy.wait()
+    last = lax.rem(owners[hops], per)
+    for j in range(1, per):
+        for sub in range(lanes):
+            add_up(lax.rem(last + j, per), sub)
+    for sub in range(lanes):
+        finish(DOWN, sub)
+        block(k, owners[hops], sub)
+    for sub in range(lanes):
+        add_up(last, sub)
+
+    turned = jnp.transpose(stat[...])
+    stat_out[...] = jnp.broadcast_to(jnp.sum(turned, axis=0, keepdims=True), stat_out.shape)
+    stats = []
+    for d in range(1, tp):
+        copy = pltpu.make_async_remote_copy(
+            src_ref=stat_out,
+            dst_ref=stat_in.at[d],
+            send_sem=st_send.at[d],
+            recv_sem=st_recv.at[d],
+            device_id={"fs": me_fs, "tp": lax.rem(me + d, tp)},
+            device_id_type=MESH,
+        )
+        copy.start()
+        stats.append(copy)
     for copy in started:
         copy.wait_send()
     for copy in inners:
         copy.wait_send()
-    for copy in firsts:
-        copy.wait()
+    if cores > 1:
+        swap.wait_send()
     for d, copy in sums:
         @pl.when(d != 0)
         def _(copy=copy):
             copy.wait_send()
+    for copy in stats:
+        copy.wait()
+    squares = stat_out[...]
     for d in range(1, tp):
-        for local in range(per):
-            lc = pl.ds(local * cols, cols)
-            pltpu.make_async_remote_copy(
-                src_ref=blocks.at[0],
-                dst_ref=parts.at[d, :, lc],
-                send_sem=rs_send.at[0],
-                recv_sem=rs_recv.at[d * per + local],
-                device_id={"fs": me_fs, "tp": lax.rem(me + d, tp)},
-                device_id_type=MESH,
-            ).wait_recv()
-
-    @pl.loop(0, seq // 64)
+        squares = squares + stat_in[d]
+    factor = lax.rsqrt(squares / width + EPS)
+    stat[...] = jnp.transpose(jnp.broadcast_to(factor[0:1], (128, seq)))
+
+    @pl.loop(0, seq // 128)
     def _(i):
-        r = pl.ds(pl.multiple_of(i * 64, 64), 64)
-        total = parts[0, r, :].astype(jnp.float32)
-        for d in range(1, tp):
-            total = total + parts[d, r, :].astype(jnp.float32)
-        out_ref[r, :] = fcols[r, :].astype(jnp.float32) + total
+        r = pl.ds(pl.multiple_of(i * 128, 128), 128)
+        out_ref[r, :] = (total[r, :] * stat[r, 0:1] * gout_ref[...]).astype(jnp.bfloat16)
 
 
 def local(order, tokens, pool_weight, pool_scale, gain_mix, gain_mlp, w_up, w_down, gain_out):
@@ -348,10 +424,11 @@
     bf, f32 = jnp.bfloat16, jnp.float32
     vmem = pl.BlockSpec(memory_space=pltpu.VMEM)
     dma = pltpu.SemaphoreType.DMA
-    second_sum = pl.pallas_call(
+    lanes = 2 if cols % 256 == 0 else 1
+    return pl.pallas_call(
         functools.partial(kernel, n, tp, order),
-        out_shape=jax.ShapeDtypeStruct((seq, own), f32),
-        in_specs=[vmem] * 7,
+        out_shape=jax.ShapeDtypeStruct((seq, own), bf),
+        in_specs=[vmem] * 8,
         out_specs=vmem,
         scratch_shapes=[
             pltpu.VMEM((pool_weight.shape[0], pool_weight.shape[1] * n, pool_weight.shape[2]), bf),
@@ -362,21 +439,29 @@
             pltpu.VMEM((seq, width), bf),
             pltpu.VMEM((seq, hid), bf),
             pltpu.VMEM((seq, own), bf),
-            pltpu.VMEM((n, seq, cols), bf),
-            pltpu.VMEM((tp, seq, own), bf),
+            pltpu.VMEM((n, lanes, seq, cols // lanes), bf),
+            pltpu.VMEM((tp, n // tp, lanes, seq, cols // lanes), bf),
             pltpu.VMEM((HALO, width), bf),
             pltpu.VMEM((HALO, width), bf),
             pltpu.VMEM((2, HALO, width), bf),
-            dma((12 * (n // 2),)),
-            dma((12 * (n // 2),)),
+            pltpu.VMEM((seq, own), f32),
+            pltpu.VMEM((seq, 128), f32),
+            pltpu.VMEM((8, seq), f32),
+            pltpu.VMEM((tp, 8, seq), f32),
+            dma((12 * (n // 2) + 2 * lanes,)),
+            dma((12 * (n // 2) + 2 * lanes,)),
             dma((tp,)),
             dma((tp,)),
             dma((tp,)),
             dma((tp,)),
             dma((2,)),
             dma((2,)),
-            dma((n,)),
-            dma((n,)),
+            dma((n * lanes,)),
+            dma((n * lanes,)),
+            dma,
+            dma,
+            dma((tp,)),
+            dma((tp,)),
         ],
         compiler_params=pltpu.CompilerParams(
             collective_id=0, has_side_effects=True, vmem_limit_bytes=63 * 1024 * 1024
@@ -384,10 +469,8 @@
     )(
         tokens, pool_weight, w_up, w_down,
         pool_scale.reshape(1, -1), gain_mix.reshape(1, -1), gain_mlp.reshape(1, -1),
+        gain_out.reshape(1, -1),
     )
-    squares = lax.psum(jnp.sum(second_sum * second_sum, axis=1), "tp")
-    scaled = second_sum * lax.rsqrt(squares / width + EPS)[:, None] * gain_out
-    return scaled.astype(jnp.bfloat16)
 
 
 def grid_width(mesh):

time: 216 us -> 205 us (0.949)
  blocking collectives: 20.4 us -> 0 us
  Pallas kernels: 192 us -> 201 us
  other arithmetic: 3.18 us -> 0 us
  local copies, waits for them, and re-layouts: 0.01 us -> 2.26 us
    psum x1 -> x0, blocking collectives: 20.4 us -> none  [local(): squares = lax.psum(jnp.sum(second_sum * second_sum, axis=1), 'tp')]
    pallas_call x1, Pallas kernels: 192 us -> 201 us  [local(): pl.pallas_call(functools.partial(kernel, n, tp, order), out_shape=jax.Sha...]
    unnamed x4 -> x1, local copies, waits for them, and re-layouts: 0.01 us -> 2.26 us
where the time goes in v2:
time: 205 us; the launch traced here: 203 us
  Pallas kernels  201 us (98%)
  local copies, waits for them, and re-layouts  2.26 us (1%)
    pallas_call x1, Pallas kernels, local(): pl.pallas_call(functools.partial(kernel, n, tp, order), out_shape=jax.Sha...  201 us

profile of v2, /device:TPU:0, one launch (start us, length us, event | category | flops | bytes accessed | tf_op | source)
XLA Modules:
  0.0 203.2 jit_solution(11824925044379597436)
XLA Ops:
  0.0 200.9 %shard_map.82 = bf16[1024,512]{1,0:T(8,128)(2,1)} custom-call(bf16[256,2048]{1,0:T(8,128)(2,1)} %tok_ref.1, bf16[4,64,512]{2,1,0:T(8,128)(2,1)} %pool_ref.1, bf16[2048,256]{1,0:T(8,128)(2,1)} %up_ref.1, bf16[2048,256]{1,0:T(8,128)(2,1)} %down_ref.1, f32[1,2048]{1,0:T(1,128)} %bitcast.4, f32[1,2048]{1,0:T(1,128)} %bitcast.5, f32[1,2048]{1,0:T(1,128)} %bitcast.6, ...), custom_call_target="tpu_custom_call" | custom-call | tf_op jit(solution)/shard_map/pallas_call | solution.py:428
  200.9 2.3 %copy.10 = bf16[1024,512]{1,0:T(8,128)(2,1)} copy(bf16[1024,512]{1,0:T(8,128)(2,1)} %shard_map.82) | data formatting | bytes 2097152
